TPU v7x, 256 devices: a whole 4x4x8 slice. The times are simulated.
256 devices in a mesh: ep: 64 (over z, y, core), tp: 4 (over x).
Axes of the slice: x: 4, y: 4, z: 8, core: 2. Of those that a mesh axis runs over, the one named last changes fastest.
Arguments:
- queries: bfloat16 [12288, 8, 128], P('ep', 'tp'), may hold values from -140 to 140
- keys: bfloat16 [12288, 4, 128], P('ep', 'tp'), may hold values from -6 to 6
- values: bfloat16 [12288, 4, 128], P('ep', 'tp'), may hold values from -6 to 6
- mix_scale: float32 [8], P('tp'), may hold values from 0.3 to 0.8
- head_gain: float32 [128], replicated, may hold values from 0.1 to 1.9
- out_weight: bfloat16 [8, 128, 2048], P('tp'), may hold values from -0.1875 to 0.1875
- moe_input: bfloat16 [24576, 2048], P(('ep', 'tp')), may hold values from -6 to 6
- norm_gain: float32 [2048], replicated, may hold values from 0.1 to 1.9
- routes: int32 [24576, 2], P(('ep', 'tp')), may hold values from 0 to 63, all different within a row; in each aligned block of 96 rows (0 to 95, 96 to 191, ...) at most 4 rows name the same one
- route_weights: float32 [24576, 2], P(('ep', 'tp')), may hold values from 0.2 to 1
- gate_weight: bfloat16 [64, 2048, 3584], P('ep', None, 'tp'), may hold values from -0.125 to 0.125
- up_weight: bfloat16 [64, 2048, 3584], P('ep', None, 'tp'), may hold values from -0.125 to 0.125
- down_weight: bfloat16 [64, 3584, 2048], P('ep', 'tp'), may hold values from -0.09375 to 0.09375
Outputs:
- attn_out: bfloat16 [12288, 2048], P(('ep', 'tp'))
- moe_out: bfloat16 [24576, 2048], P(('ep', 'tp'))
Inputs may be any that keep to these rules, and one draw needn't show every extreme that they name: `routes`: the 2 experts of a row differ. In each aligned block of 96 rows (the rows of one device) no expert is named by more than 4 rows, and in some blocks an expert is named by exactly 4 rows.
All inputs are finite; a program needn't handle non-finite values.
Results may differ from a plain program's by a relative error of at most 0.014.
Values may be sent and summed in bfloat16 or wider, within the bound.
A program may use at most 128 MiB of HBM per device.

v0:
```python
import math
import jax
import jax.numpy as jnp
from jax import lax
from jax.sharding import Mesh
from jax.sharding import PartitionSpec as P

EP = ("ep_0", "ep_1", "ep_2")
EP_TP = ("ep_0", "ep_1", "ep_2", "tp")
NEG_LARGE = -1e30


def joined_along(tiles, dim):
    tiles = jnp.moveaxis(tiles, 0, dim)
    lengths = tiles.shape
    return tiles.reshape(*lengths[:dim], lengths[dim] * lengths[dim + 1], *lengths[dim + 2 :])


def gather_in_order(value, axes, order):
    tiles = value[None]
    for k in order:
        tiles = lax.all_gather(tiles, axes[k], axis=0, tiled=True)
    current = [lax.axis_size(axes[k]) for k in reversed(order)]
    tiles = tiles.reshape(*current, *value.shape)
    turned = sorted(range(len(order)), key=lambda place: order[len(order) - 1 - place])
    return tiles.transpose(*turned, *range(len(order), tiles.ndim)).reshape(-1, *value.shape)


def gathered_by_axis(value, axes, order, dim):
    return joined_along(gather_in_order(value, axes, order), dim)


def split_up(value, dim, peers):
    before, after = (value.shape[:dim], value.shape[dim + 1 :])
    return jnp.moveaxis(value.reshape(*before, peers, -1, *after), dim, 0)


def summed_on_arrival(value, axis, dim):
    peers = lax.axis_size(axis)
    tiles = lax.all_to_all(split_up(value, dim, peers), axis, 0, 0, tiled=True)
    return jnp.sum(tiles.astype(jnp.float32), axis=0)


def attend_update(running, query_set, positions, key_block, value_block, key_anchor, scaling):
    row_peak, totals, numerator = running
    span = key_block.shape[0]
    scores = (
        jnp.einsum("tkgmd,skmd->kgmts", query_set, key_block, preferred_element_type=jnp.float32)
        * scaling
    )
    visible = (key_anchor + jnp.arange(span, dtype=jnp.int32))[None, :] <= positions[:, None]
    scores = jnp.where(visible, scores, NEG_LARGE)
    new_peak = jnp.maximum(row_peak, jnp.max(scores, axis=-1))
    weights = jnp.where(visible, jnp.exp(scores - new_peak[..., None]), 0.0)
    factor = jnp.exp(row_peak - new_peak)
    totals = totals * factor + jnp.sum(weights, axis=-1)
    numerator = numerator * factor[..., None] + jnp.einsum(
        "rnouf,frj->rnouj",
        weights.astype(jnp.bfloat16),
        value_block,
        preferred_element_type=jnp.float32,
    )
    return (new_peak, totals, numerator)


def body(
    queries,
    keys,
    values,
    mix_scale,
    head_gain,
    out_weight,
    moe_input,
    norm_gain,
    routes,
    route_weights,
    gate_weight,
    up_weight,
    down_weight,
):
    rows_here = queries.shape[0]
    key_heads = keys.shape[1]
    head_count = queries.shape[1]
    group_size = head_count // key_heads
    head_dim = queries.shape[2] // 2
    value_dim = values.shape[2]
    ep_size = lax.axis_size(EP)
    own_start = lax.axis_index(EP) * rows_here
    grouped = queries.reshape(rows_here, key_heads, group_size, 2, head_dim)
    own_positions = own_start + jnp.arange(rows_here, dtype=jnp.int32)
    query_sets = ((grouped, own_positions),)
    scaling = 1.0 / math.sqrt(head_dim)

    def empty_state(row_total):
        return (
            jnp.full((key_heads, group_size, 2, row_total), NEG_LARGE, jnp.float32),
            jnp.zeros((key_heads, group_size, 2, row_total), jnp.float32),
            jnp.zeros((key_heads, group_size, 2, row_total, value_dim), jnp.float32),
        )

    initial = tuple((empty_state(entry[0].shape[0]) for entry in query_sets))
    key_rows = gathered_by_axis(keys, EP, (1, 0, 2), 0)
    value_rows = gathered_by_axis(values, EP, (1, 0, 2), 0)
    length = key_rows.shape[0]
    span = length
    while span > 1024 and span % 2 == 0:
        span = span // 2
    key_rows = key_rows.reshape(length, key_heads, 2, head_dim)

    def sweep(step_id, states):
        anchor = step_id * span
        key_block = lax.dynamic_slice_in_dim(key_rows, step_id * span, span, 0)
        value_block = lax.dynamic_slice_in_dim(value_rows, step_id * span, span, 0)
        updated = []
        for (query_set, positions), status in zip(query_sets, states):

            def advance(current):
                return attend_update(
                    current, query_set, positions, key_block, value_block, anchor, scaling
                )

            def unchanged(current):
                return current

            updated.append(lax.cond(anchor <= positions[-1], advance, unchanged, status))
        return tuple(updated)

    folded = lax.fori_loop(0, length // span, sweep, initial)
    mixing = mix_scale.reshape(key_heads, group_size, 1, 1)
    outputs = []
    for status in folded:
        row_peak, totals, numerator = status
        blended = numerator[:, :, 0] / totals[:, :, 0, :, None] - mixing * (
            numerator[:, :, 1] / totals[:, :, 1, :, None]
        )
        normed = (
            blended
            * lax.rsqrt(jnp.mean(blended * blended, axis=-1, keepdims=True) + 1e-05)
            * head_gain
        )
        outputs.append(
            jnp.transpose(normed.astype(jnp.bfloat16), (2, 0, 1, 3)).reshape(
                -1, head_count * value_dim
            )
        )
    head_flat = outputs[0]
    weight_flat = out_weight.reshape(head_count * value_dim, -1)
    widened = moe_input.astype(jnp.float32)
    normed_in = (
        widened * lax.rsqrt(jnp.mean(widened * widened, axis=-1, keepdims=True) + 1e-06) * norm_gain
    ).astype(jnp.bfloat16)
    tok_count = moe_input.shape[0]
    top_count = routes.shape[1]
    experts = ep_size * gate_weight.shape[0]
    capacity = max(2, 3 * top_count * tok_count // (2 * experts))
    flattened = routes.reshape(-1)
    one_hot = (flattened[:, None] == jnp.arange(experts, dtype=jnp.int32)[None, :]).astype(
        jnp.int32
    )
    before = jnp.cumsum(one_hot, axis=0) - one_hot
    ranking = jnp.sum(before * one_hot, axis=1)
    slot_ids = (flattened * capacity + ranking).reshape(tok_count, top_count)
    slot_total = experts * capacity
    dispatch = jnp.any(
        jnp.arange(slot_total, dtype=jnp.int32)[:, None, None] == slot_ids[None], axis=2
    ).astype(jnp.bfloat16)
    outbound = jnp.dot(dispatch, normed_in, preferred_element_type=jnp.float32).astype(jnp.bfloat16)
    received = lax.all_to_all(outbound, EP, split_axis=0, concat_axis=0, tiled=True)
    inputs = lax.all_gather(received, "tp", axis=0, tiled=True)
    gate_proj = jnp.dot(inputs, gate_weight[0], preferred_element_type=jnp.float32)
    up_proj = jnp.dot(inputs, up_weight[0], preferred_element_type=jnp.float32)
    hidden_all = (jax.nn.silu(gate_proj) * up_proj).astype(jnp.bfloat16)
    attn_out = summed_on_arrival(
        jnp.dot(head_flat, weight_flat, preferred_element_type=jnp.float32).astype(jnp.bfloat16),
        "tp",
        0,
    ).astype(jnp.bfloat16)
    expert_out = summed_on_arrival(
        jnp.dot(hidden_all, down_weight[0], preferred_element_type=jnp.float32).astype(
            jnp.bfloat16
        ),
        "tp",
        0,
    ).astype(jnp.bfloat16)
    returned_rows = lax.all_to_all(expert_out, EP, split_axis=0, concat_axis=0, tiled=True)
    picked = jnp.take(returned_rows, slot_ids, axis=0)
    moe_out = jnp.sum(route_weights[:, :, None] * picked.astype(jnp.float32), axis=1).astype(
        jnp.bfloat16
    )
    return (attn_out, moe_out)


def solution(mesh):
    split = Mesh(mesh.devices.reshape(8, 4, 2, mesh.shape["tp"]), ("ep_0", "ep_1", "ep_2", "tp"))
    placed = (
        P(EP, "tp", None),
        P(EP, "tp", None),
        P(EP, "tp", None),
        P("tp"),
        P(),
        P("tp", None, None),
        P(EP_TP, None),
        P(),
        P(EP_TP, None),
        P(EP_TP, None),
        P(EP, None, "tp"),
        P(EP, None, "tp"),
        P(EP, "tp", None),
    )
    return jax.shard_map(
        body,
        mesh=split,
        in_specs=placed,
        out_specs=(P(EP_TP, None), P(EP_TP, None)),
        check_vma=False,
    )
```

profile of v0, /device:TPU:1, one launch (start us, length us, event | category | flops | bytes accessed | tf_op | source)
XLA Modules:
  0.0 368.3 jit_solution(15211746906782629320)
XLA Ops:
  7.2 12.6 %all-gather = bf16[768,1,128]{2,0,1:T(8,128)(2,1)} all-gather(bf16[192,1,128]{2,0,1:T(8,128)(2,1)} %param.18), channel_id=2, replica_groups=mesh['ep_0'=8,'ep_1'=4,'ep_2'=2,'tp'=4] {'ep_1'}, dimensions={0}, use_global_device_ids=true | all-gather | bytes 245760 | tf_op jit(solution)/shard_map/all_gather | solution.py:22
  19.9 10.2 %all-gather.1 = bf16[768,1,128]{2,0,1:T(8,128)(2,1)} all-gather(bf16[192,1,128]{2,0,1:T(8,128)(2,1)} %param.19), channel_id=3, replica_groups=mesh['ep_0'=8,'ep_1'=4,'ep_2'=2,'tp'=4] {'ep_1'}, dimensions={0}, use_global_device_ids=true | all-gather | bytes 245760 | tf_op jit(solution)/shard_map/all_gather | solution.py:22
  30.2 0.8 copy.86
  31.0 0.1 eq.35
  31.1 0.6 reduce-window.6
  31.7 0.2 slice_reduce_fusion
  32.1 0.1 reduce_sum.76
  32.3 0.7 compare_and_fusion
  33.1 1.2 fusion.22
  34.3 1.5 convolution_convert_fusion.1
  35.8 0.4 all_to_all.23
  36.3 47.2 %all_to_all.34 = bf16[64,4,2048]{2,1,0:T(4,128)(2,1)S(1)} all-to-all(bf16[64,4,2048]{2,1,0:T(4,128)(2,1)S(1)} %all_to_all.23), channel_id=1, replica_groups=mesh['ep_0'=8,'ep_1'=4,'ep_2'=2,'tp'=4] {'ep_0','ep_1','ep_2'}, dimensions={0} | all-to-all | bytes 2097152 | tf_op jit(solution)/shard_map/all_to_all | solution.py:168
  83.5 1.1 all_to_all.25
  84.7 0.5 all-gather.10.cloned.1.call-update
  85.2 23.4 %all-gather.12.cloned.1.call-done = bf16[32,192,1,128]{3,1,2,0:T(8,128)(2,1)} async-done(((bf16[4,192,1,128]{3,1,2,0:T(8,128)(2,1)}), bf16[32,192,1,128]{3,1,2,0:T(8,128)(2,1)}) %all-gather.12.cloned.1.call-update) | async-done | bytes 1572880 | tf_op jit(solution)/shard_map/all_gather | solution.py:22
  108.7 54.8 %all-gather.16.cloned.1.call-done = bf16[1024,2048]{1,0:T(8,128)(2,1)} async-done(((bf16[256,2048]{1,0:T(8,128)(2,1)}), bf16[1024,2048]{1,0:T(8,128)(2,1)}) %all-gather.16.cloned.1.call-update) | async-done | bytes 4194320 | tf_op jit(solution)/shard_map/all_gather | solution.py:169
  163.5 7.5 %fusion.16 = f32[1024,896]{1,0:T(8,128)S(1)} fusion(bf16[1024,2048]{1,0:T(8,128)(2,1)} %all-gather.16.cloned.1.call-done, bf16[1,2048,896]{2,1,0:T(8,128)(2,1)} %param.28), kind=kOutput, calls=%fused_computation.26 | convolution fusion | flops 3758096384 | bytes 11534336 | tf_op jit(solution)/shard_map/dot_general | solution.py:171
  171.0 4.7 %multiply_convert_fusion = bf16[1024,896]{1,0:T(8,128)(2,1)S(1)} fusion(f32[1024,896]{1,0:T(8,128)S(1)} %fusion.16, bf16[1024,2048]{1,0:T(8,128)(2,1)S(1)} %copy-done.5, bf16[1,2048,896]{2,1,0:T(8,128)(2,1)S(1)} %copy-done.6), kind=kOutput, calls=%fused_computation.30 | convolution fusion | flops 3763601408 | bytes 13369344 | tf_op jit(solution)/shard_map/dot_general | solution.py:170
  175.8 6.1 %convolution_convert_fusion = bf16[1024,2048]{1,0:T(8,128)(2,1)} fusion(bf16[1024,896]{1,0:T(8,128)(2,1)S(1)} %multiply_convert_fusion, bf16[1,896,2048]{2,1,0:T(8,128)(2,1)S(1)} %copy-done.7), kind=kOutput, calls=%fused_computation.24 | convolution fusion | flops 3760193536 | bytes 9699328 | tf_op jit(solution)/shard_map/dot_general | solution.py:179
  181.9 5.1 %all-to-all-start.2 = ((bf16[4,256,2048]{2,1,0:T(8,128)(2,1)}), bf16[4,256,2048]{2,1,0:T(8,128)(2,1)}, u32[]{:S(2)}, u32[]{:S(2)}) async-start(bf16[4,256,2048]{2,1,0:T(8,128)(2,1)} %bitcast.121), calls=%async_computation.2 | async-start | bytes 8388608 | tf_op jit(solution)/shard_map/all_to_all | solution.py:40
  187.1 0.1 copy.80
  187.2 11.2 %copy.79 = bf16[8,4,2,192,1,128]{3,2,1,0,5,4:T(2,128)(2,1)} copy(bf16[8,4,2,192,1,128]{5,3,1,0,2,4:T(8,128)(2,1)} %bitcast.122) | data formatting | bytes 6291456 | tf_op jit(solution)/shard_map/transpose | solution.py:26
  198.4 9.9 %reshape_reshape_reshape.3 = bf16[12288,1,2,64]{0,3,2,1:T(8,128)(2,1)} reshape(bf16[8,4,2,192,1,128]{3,2,1,0,5,4:T(2,128)(2,1)} %copy.79) | data formatting | bytes 6291456 | tf_op jit(solution)/shard_map/reshape;reshape;reshape | solution.py:108
  208.4 3.9 %copy.81 = bf16[8,4,2,192,1,128]{5,3,2,1,0,4:T(8,128)(2,1)} copy(bf16[8,4,2,192,1,128]{5,3,1,0,2,4:T(8,128)(2,1)} %bitcast.124) | data formatting | bytes 6291456 | tf_op jit(solution)/shard_map/transpose | solution.py:26
  212.3 24.4 %while.17 = (s32[]{:T(128)}, f32[1,2,2,192]{3,1,2,0:T(2,128)S(1)}, f32[1,2,2,192]{3,1,2,0:T(2,128)S(1)}, f32[1,2,2,192,128]{4,3,2,1,0:T(8,128)S(1)}, s32[192]{0:...) while((s32[]{:T(128)}, f32[1,2,2,192]{3,1,2,0:T(2,128)S(1)}, ...), condition=%wide.region_5.6_spmd, body=%wide.region_0.5_spmd.sunk | while | flops 232147968 | bytes 8857645 | solution.py:128
  212.4 0.6 slice.57
  213.6 4.3 %conditional.2 = ((f32[1,2,2,192]{3,1,2,0:T(2,128)S(1)}, f32[1,2,2,192]{3,1,2,0:T(2,128)S(1)}, f32[1,2,2,192,128]{4,3,2,1,0:T(8,128)S(1)})) conditional(s32[]{:T(128)} %convert_element_type.91, (f32[1,2,2,192]{3,1,2,0:T(2,128)S(1)}, f32[1,2,2,192]{3,1,2,0:T(2,128)S(1)}, f32[1,2,2,192,128]{4,3,2,1,0:T(8,128)S(1)}) %tuple.61, (s32[]{:T(128)}, ...), branch_computations={%region_1.0_spmd, %region_2.4_spmd} | conditional | flops 232147968 | bytes 8857422 | solution.py:125
  213.6 0.1 broadcast_compare_fusion
  213.8 1.6 fusion
  215.4 0.9 fusion.4
  216.3 1.5 fusion.3
  217.9 0.6 slice.57
  219.1 0.6 slice.57
  220.4 0.6 slice.57
  221.7 0.6 slice.57
  222.9 0.6 slice.57
  224.2 0.6 slice.57
  225.4 0.6 slice.57
  226.7 0.6 slice.57
  227.9 0.6 slice.57
  229.2 0.6 slice.57
  230.4 0.6 slice.57
  231.7 0.6 slice.57
  233.0 0.6 slice.57
  234.2 0.6 slice.57
  235.5 0.6 slice.57
  236.7 0.3 multiply_reduce_fusion.1
  237.1 0.1 fusion.32
  237.3 1.3 convolution_convert_fusion.2
  238.6 4.0 %all-to-all-start = ((bf16[4,48,2048]{2,1,0:T(8,128)(2,1)}), bf16[4,48,2048]{2,1,0:T(8,128)(2,1)S(1)}, u32[]{:S(2)}, u32[]{:S(2)}) async-start(bf16[4,48,2048]{2,1,0:T(8,128)(2,1)} %bitcast.30), calls=%async_computation | async-start | bytes 1572864 | tf_op jit(solution)/shard_map/all_to_all | solution.py:40
  242.6 3.1 reduce_sum.78
  245.7 1.2 all_to_all.27
  246.9 6.6 %all-to-all-done = bf16[4,48,2048]{2,1,0:T(8,128)(2,1)S(1)} async-done(((bf16[4,48,2048]{2,1,0:T(8,128)(2,1)}), bf16[4,48,2048]{2,1,0:T(8,128)(2,1)S(1)}, u32[]{:S(2)}, u32[]{:S(2)}) %all-to-all-start) | async-done | bytes 786464 | tf_op jit(solution)/shard_map/all_to_all | solution.py:40
  253.5 74.0 %all-to-all-start.3 = ((bf16[64,4,2048]{2,1,0:T(4,128)(2,1)}), bf16[64,4,2048]{2,1,0:T(4,128)(2,1)S(1)}, u32[]{:S(2)}, u32[]{:S(2)}) async-start(bf16[64,4,2048]{2,1,0:T(4,128)(2,1)} %all_to_all.27), calls=%async_computation.3 | async-start | bytes 2097152 | tf_op jit(solution)/shard_map/all_to_all | solution.py:185
  327.5 0.1 copy.91
  327.6 0.1 reshape.218
  327.7 0.1 copy.90
  327.9 0.1 copy.85
  328.0 0.8 reduce_sum.74
  328.8 26.8 %all-to-all-done.3 = bf16[64,4,2048]{2,1,0:T(4,128)(2,1)S(1)} async-done(((bf16[64,4,2048]{2,1,0:T(4,128)(2,1)}), bf16[64,4,2048]{2,1,0:T(4,128)(2,1)S(1)}, u32[]{:S(2)}, u32[]{:S(2)}) %all-to-all-start.3) | async-done | bytes 1048608 | tf_op jit(solution)/shard_map/all_to_all | solution.py:185
  355.6 0.3 all_to_all.29
  355.9 1.1 gather_fusion
  357.1 0.5 reshape.217
  357.6 4.2 %multiply_reduce_fusion = bf16[96,2048]{1,0:T(8,128)(2,1)} fusion(bf16[96,2,2048]{2,1,0:T(2,128)(2,1)S(1)} %reshape.217, pred[96,2]{1,0:T(8,128)(4,1)S(1)} %copy.90, f32[96,2]{1,0:T(8,128)S(1)} %copy.85), kind=kLoop, calls=%fused_computation.33 | loop fusion | flops 1376256 | bytes 1180608 | tf_op jit(solution)/shard_map/reduce_sum | solution.py:187
  (68 shorter events, 1.1 us)
Async XLA Ops:
  7.2 230.1 %copy-start = (bf16[2,128,2048]{2,1,0:T(8,128)(2,1)S(1)}, bf16[2,128,2048]{2,1,0:T(8,128)(2,1)}, u32[]{:S(2)}) copy-start(bf16[2,128,2048]{2,1,0:T(8,128)(2,1)} %param.22) | copy-start | bytes 3145732
  7.2 77.5 %all-gather.8.cloned.1.call-start = ((), (), s32[]{:S(2)}) async-start(), calls=%async_computation.4 | async-start | bytes 1769472 | tf_op jit(solution)/shard_map/all_gather | solution.py:22
  19.9 88.8 %all-gather.12.cloned.1.call-start = ((), (), s32[]{:S(2)}) async-start(), calls=%async_computation.6 | async-start | bytes 1769472 | tf_op jit(solution)/shard_map/all_gather | solution.py:22
  30.1 133.4 %all-gather.16.cloned.1.call-start = ((), (), s32[]{:S(2)}) async-start(), calls=%async_computation.8 | async-start | bytes 5242880 | tf_op jit(solution)/shard_map/all_gather | solution.py:169
  84.6 102.6 %all-gather.10.cloned.1.call-start = ((), (), s32[]{:S(2)}) async-start(), calls=%async_computation.5 | async-start | bytes 4718592 | tf_op jit(solution)/shard_map/all_gather | solution.py:22
  85.2 123.2 %all-gather.14.cloned.1.call-start = ((), (), s32[]{:S(2)}) async-start(), calls=%async_computation.7 | async-start | bytes 4718592 | tf_op jit(solution)/shard_map/all_gather | solution.py:22
  163.5 7.5 %copy-start.5 = (bf16[1024,2048]{1,0:T(8,128)(2,1)S(1)}, bf16[1024,2048]{1,0:T(8,128)(2,1)}, u32[]{:S(2)}) copy-start(bf16[1024,2048]{1,0:T(8,128)(2,1)} %all-gather.16.cloned.1.call-done) | copy-start | bytes 12582916
  163.5 7.5 %copy-start.6 = (bf16[1,2048,896]{2,1,0:T(8,128)(2,1)S(1)}, bf16[1,2048,896]{2,1,0:T(8,128)(2,1)}, u32[]{:S(2)}) copy-start(bf16[1,2048,896]{2,1,0:T(8,128)(2,1)} %param.27) | copy-start | bytes 11010052
  171.0 4.8 %copy-start.7 = (bf16[1,896,2048]{2,1,0:T(8,128)(2,1)S(1)}, bf16[1,896,2048]{2,1,0:T(8,128)(2,1)}, u32[]{:S(2)}) copy-start(bf16[1,896,2048]{2,1,0:T(8,128)(2,1)} %param.29) | copy-start | bytes 11010052
  181.9 5.2 %copy-start.1 = (bf16[192,2,128]{2,1,0:T(2,128)(2,1)S(1)}, bf16[192,2,128]{2,1,0:T(2,128)(2,1)}, u32[]{:S(2)}) copy-start(bf16[192,2,128]{2,1,0:T(2,128)(2,1)} %param.17) | copy-start | bytes 294916
  181.9 56.7 %all-to-all-start.2 = ((bf16[4,256,2048]{2,1,0:T(8,128)(2,1)}), bf16[4,256,2048]{2,1,0:T(8,128)(2,1)}, u32[]{:S(2)}, u32[]{:S(2)}) async-start(bf16[4,256,2048]{2,1,0:T(8,128)(2,1)} %bitcast.121), calls=%async_computation.2 | async-start | bytes 8388608 | tf_op jit(solution)/shard_map/all_to_all | solution.py:40
  212.3 24.4 %copy-start.4 = (f32[2]{0:T(128)S(1)}, f32[2]{0:T(128)}, u32[]{:S(2)}) copy-start(f32[2]{0:T(128)} %param.20) | copy-start | bytes 28
  212.3 24.7 %copy-start.3 = (f32[128]{0:T(128)S(1)}, f32[128]{0:T(128)}, u32[]{:S(2)}) copy-start(f32[128]{0:T(128)} %param.21) | copy-start | bytes 1540
  238.6 14.9 %all-to-all-start = ((bf16[4,48,2048]{2,1,0:T(8,128)(2,1)}), bf16[4,48,2048]{2,1,0:T(8,128)(2,1)S(1)}, u32[]{:S(2)}, u32[]{:S(2)}) async-start(bf16[4,48,2048]{2,1,0:T(8,128)(2,1)} %bitcast.30), calls=%async_computation | async-start | bytes 1572864 | tf_op jit(solution)/shard_map/all_to_all | solution.py:40
  245.7 82.2 %copy-start.2 = (f32[96,2]{0,1:T(2,128)S(1)}, f32[96,2]{0,1:T(2,128)}, u32[]{:S(2)}) copy-start(f32[96,2]{0,1:T(2,128)} %param.26) | copy-start | bytes 2308
  253.5 102.2 %all-to-all-start.3 = ((bf16[64,4,2048]{2,1,0:T(4,128)(2,1)}), bf16[64,4,2048]{2,1,0:T(4,128)(2,1)S(1)}, u32[]{:S(2)}, u32[]{:S(2)}) async-start(bf16[64,4,2048]{2,1,0:T(4,128)(2,1)} %all_to_all.27), calls=%async_computation.3 | async-start | bytes 2097152 | tf_op jit(solution)/shard_map/all_to_all | solution.py:185
Sparse Core Ops, SparseCore 0:
  20.0 43.5 all-gather.7
  65.3 43.2 all-gather.11
  110.5 52.9 all-gather.15
  165.2 18.7 all-gather.9
  185.6 18.7 all-gather.13
where the time goes:
time: 370 us; the launch traced here: 368 us
  waiting for transfers between devices  112 us (30%)
  starting transfers between devices  83.3 us (23%)
  blocking collectives  70 us (19%)
  local copies, waits for them, and re-layouts  41.2 us (11%)
  matrix products  24.3 us (7%)
  between operations  14.1 us (4%)
  other arithmetic  12.4 us (3%)
  loops' own time  10.7 us (3%)
    all_to_all x1, starting transfers between devices, body(): lax.all_to_all(expert_out, EP, split_axis=0, concat_axis=0, tiled=True)  74 us
    all_gather x1, waiting for transfers between devices, body(): inputs = lax.all_gather(received, 'tp', axis=0, tiled=True)  54.8 us
    all_to_all x1, blocking collectives, body(): lax.all_to_all(outbound, EP, split_axis=0, concat_axis=0, tiled=True)  47.2 us
    all_to_all x1, waiting for transfers between devices, body(): lax.all_to_all(expert_out, EP, split_axis=0, concat_axis=0, tiled=True)  26.8 us
    all_gather x4, waiting for transfers between devices, gather_in_order(): tiles = lax.all_gather(tiles, axes[k], axis=0, tiled=True)  23.5 us
    all_gather x2, blocking collectives, gather_in_order(): tiles = lax.all_gather(tiles, axes[k], axis=0, tiled=True)  22.8 us
    transpose x2, local copies, waits for them, and re-layouts, gather_in_order(): tiles.transpose(*turned, *range(len(order), tiles.ndim))  15.1 us
    another operation x1, loops' own time, body(): folded = lax.fori_loop(0, length // span, sweep, initial)  10.4 us
  transfers between devices with their start and end apart: 8, of which 4 were waited for; matrix products, arithmetic and copies ran while one was open for 19% of the time, Pallas kernels for 0%

commit v1 on v0

--- a/solution.py
+++ b/solution.py
@@ -166,7 +166,11 @@
     ).astype(jnp.bfloat16)
     outbound = jnp.dot(dispatch, normed_in, preferred_element_type=jnp.float32).astype(jnp.bfloat16)
     received = lax.all_to_all(outbound, EP, split_axis=0, concat_axis=0, tiled=True)
-    inputs = lax.all_gather(received, "tp", axis=0, tiled=True)
+    length_2 = lax.axis_size("tp")
+    repeats = [length_2 if d == 0 else 1 for d in range(received.ndim)]
+    inputs = lax.all_to_all(
+        jnp.tile(received, repeats), "tp", split_axis=0, concat_axis=0, tiled=True
+    )
     gate_proj = jnp.dot(inputs, gate_weight[0], preferred_element_type=jnp.float32)
     up_proj = jnp.dot(inputs, up_weight[0], preferred_element_type=jnp.float32)
     hidden_all = (jax.nn.silu(gate_proj) * up_proj).astype(jnp.bfloat16)

time: 370 us -> 349 us (0.943)
  waiting for transfers between devices: 112 us -> 79.8 us
  local copies, waits for them, and re-layouts: 41.2 us -> 45.7 us
    all_gather x1 -> x0, waiting for transfers between devices: 54.8 us -> none  [body(): inputs = lax.all_gather(received, 'tp', axis=0, tiled=True)]
    all_to_all x0 -> x1, waiting for transfers between devices: none -> 31.9 us  [body(): lax.all_to_all(jnp.tile(received, repeats), 'tp', split_axis=0, concat_ax...]
    all_gather x4, waiting for transfers between devices: 23.5 us -> 16.3 us  [gather_in_order(): tiles = lax.all_gather(tiles, axes[k], axis=0, tiled=True)]
    all_to_all x0 -> x1, starting transfers between devices: none -> 4.85 us  [body(): lax.all_to_all(jnp.tile(received, repeats), 'tp', split_axis=0, concat_ax...]
    another operation x2 -> x4, local copies, waits for them, and re-layouts: 0.19 us -> 4.09 us  [the longest x2 3.9 us: body(): jnp.tile(received, repeats)]
  transfers between devices with their start and end apart: 8 -> 8, of which waited for: 4 -> 4; matrix products, arithmetic and copies ran while one was open for 19% -> 22% of each run, Pallas kernels for 0% -> 0%
where the time goes in v1:
time: 349 us; the launch traced here: 347 us
  starting transfers between devices  86.3 us (25%)
  waiting for transfers between devices  79.8 us (23%)
  blocking collectives  70.1 us (20%)
  local copies, waits for them, and re-layouts  45.7 us (13%)
  matrix products  26.9 us (8%)
  between operations  14.1 us (4%)
  other arithmetic  13.5 us (4%)
  loops' own time  10.9 us (3%)
    all_to_all x1, starting transfers between devices, body(): lax.all_to_all(expert_out, EP, split_axis=0, concat_axis=0, tiled=True)  72.2 us
    all_to_all x1, blocking collectives, body(): lax.all_to_all(outbound, EP, split_axis=0, concat_axis=0, tiled=True)  47.3 us
    all_to_all x1, waiting for transfers between devices, body(): lax.all_to_all(jnp.tile(received, repeats), 'tp', split_axis=0, concat_ax...  31.9 us
    all_to_all x1, waiting for transfers between devices, body(): lax.all_to_all(expert_out, EP, split_axis=0, concat_axis=0, tiled=True)  25.7 us
    all_gather x2, blocking collectives, gather_in_order(): tiles = lax.all_gather(tiles, axes[k], axis=0, tiled=True)  22.8 us
    all_gather x4, waiting for transfers between devices, gather_in_order(): tiles = lax.all_gather(tiles, axes[k], axis=0, tiled=True)  16.3 us
    transpose x2, local copies, waits for them, and re-layouts, gather_in_order(): tiles.transpose(*turned, *range(len(order), tiles.ndim))  15.1 us
    another operation x1, loops' own time, body(): folded = lax.fori_loop(0, length // span, sweep, initial)  10.7 us
  transfers between devices with their start and end apart: 8, of which 4 were waited for; matrix products, arithmetic and copies ran while one was open for 22% of the time, Pallas kernels for 0%

profile of v1, /device:TPU:1, one launch (start us, length us, event | category | flops | bytes accessed | tf_op | source)
XLA Modules:
  0.0 347.3 jit_solution(563593959831310710)
XLA Ops:
  7.2 12.6 %all-gather = bf16[768,1,128]{2,0,1:T(8,128)(2,1)} all-gather(bf16[192,1,128]{2,0,1:T(8,128)(2,1)} %param.18), channel_id=2, replica_groups=mesh['ep_0'=8,'ep_1'=4,'ep_2'=2,'tp'=4] {'ep_1'}, dimensions={0}, use_global_device_ids=true | all-gather | bytes 245760 | tf_op jit(solution)/shard_map/all_gather | solution.py:22
  19.9 10.2 %all-gather.1 = bf16[768,1,128]{2,0,1:T(8,128)(2,1)} all-gather(bf16[192,1,128]{2,0,1:T(8,128)(2,1)} %param.19), channel_id=3, replica_groups=mesh['ep_0'=8,'ep_1'=4,'ep_2'=2,'tp'=4] {'ep_1'}, dimensions={0}, use_global_device_ids=true | all-gather | bytes 245760 | tf_op jit(solution)/shard_map/all_gather | solution.py:22
  30.2 0.8 copy.86
  31.0 0.1 eq.35
  31.1 0.6 reduce-window.6
  31.7 0.2 slice_reduce_fusion
  32.1 0.1 reduce_sum.76
  32.3 0.7 compare_and_fusion
  33.1 1.2 fusion.22
  34.3 1.5 convolution_convert_fusion.1
  35.8 0.4 all_to_all.27
  36.3 47.3 %all_to_all.40 = bf16[64,4,2048]{2,1,0:T(4,128)(2,1)} all-to-all(bf16[64,4,2048]{2,1,0:T(4,128)(2,1)S(1)} %all_to_all.27), channel_id=1, replica_groups=mesh['ep_0'=8,'ep_1'=4,'ep_2'=2,'tp'=4] {'ep_0','ep_1','ep_2'}, dimensions={0} | all-to-all | bytes 2097152 | tf_op jit(solution)/shard_map/all_to_all | solution.py:168
  83.6 1.4 tile.4
  85.0 2.5 tile.10
  87.5 4.8 %all-to-all-start.2 = ((bf16[4,256,2048]{2,1,0:T(8,128)(2,1)}), bf16[4,256,2048]{2,1,0:T(8,128)(2,1)}, u32[]{:S(2)}, u32[]{:S(2)}) async-start(bf16[4,256,2048]{2,1,0:T(8,128)(2,1)} %tile.10), calls=%async_computation.2 | async-start | bytes 8388608 | tf_op jit(solution)/shard_map/all_to_all | solution.py:171
  92.4 16.2 %all-gather.11.cloned.1.call-done = bf16[32,192,1,128]{3,1,2,0:T(8,128)(2,1)} async-done(((bf16[4,192,1,128]{3,1,2,0:T(8,128)(2,1)}), bf16[32,192,1,128]{3,1,2,0:T(8,128)(2,1)}) %all-gather.11.cloned.1.call-update) | async-done | bytes 1572880 | tf_op jit(solution)/shard_map/all_gather | solution.py:22
  108.7 31.9 %all-to-all-done.2 = bf16[4,256,2048]{2,1,0:T(8,128)(2,1)} async-done(((bf16[4,256,2048]{2,1,0:T(8,128)(2,1)}), bf16[4,256,2048]{2,1,0:T(8,128)(2,1)}, u32[]{:S(2)}, u32[]{:S(2)}) %all-to-all-start.2) | async-done | bytes 4194336 | tf_op jit(solution)/shard_map/all_to_all | solution.py:171
  140.6 7.5 %fusion.16 = f32[1024,896]{1,0:T(8,128)S(1)} fusion(bf16[1024,2048]{1,0:T(8,128)(2,1)} %bitcast.32, bf16[1,2048,896]{2,1,0:T(8,128)(2,1)} %param.28), kind=kOutput, calls=%fused_computation.26 | convolution fusion | flops 3758096384 | bytes 11534336 | tf_op jit(solution)/shard_map/dot_general | solution.py:175
  148.1 7.3 %multiply_convert_fusion = bf16[1024,896]{1,0:T(8,128)(2,1)S(1)} fusion(f32[1024,896]{1,0:T(8,128)S(1)} %fusion.16, bf16[1024,2048]{1,0:T(8,128)(2,1)} %bitcast.32, bf16[1,2048,896]{2,1,0:T(8,128)(2,1)S(1)} %copy-done.6), kind=kOutput, calls=%fused_computation.30 | convolution fusion | flops 3763601408 | bytes 13369344 | tf_op jit(solution)/shard_map/dot_general | solution.py:174
  155.5 6.1 %convolution_convert_fusion = bf16[1024,2048]{1,0:T(8,128)(2,1)} fusion(bf16[1024,896]{1,0:T(8,128)(2,1)S(1)} %multiply_convert_fusion, bf16[1,896,2048]{2,1,0:T(8,128)(2,1)S(1)} %copy-done.7), kind=kOutput, calls=%fused_computation.24 | convolution fusion | flops 3760193536 | bytes 9699328 | tf_op jit(solution)/shard_map/dot_general | solution.py:183
  161.5 5.2 %all-to-all-start.3 = ((bf16[4,256,2048]{2,1,0:T(8,128)(2,1)}), bf16[4,256,2048]{2,1,0:T(8,128)(2,1)}, u32[]{:S(2)}, u32[]{:S(2)}) async-start(bf16[4,256,2048]{2,1,0:T(8,128)(2,1)} %bitcast.122), calls=%async_computation.3 | async-start | bytes 8388608 | tf_op jit(solution)/shard_map/all_to_all | solution.py:40
  166.7 0.1 copy.80
  166.9 11.1 %copy.79 = bf16[8,4,2,192,1,128]{3,2,1,0,5,4:T(2,128)(2,1)} copy(bf16[8,4,2,192,1,128]{5,3,1,0,2,4:T(8,128)(2,1)} %bitcast.123) | data formatting | bytes 6291456 | tf_op jit(solution)/shard_map/transpose | solution.py:26
  178.0 9.8 %reshape_reshape_reshape.3 = bf16[12288,1,2,64]{0,3,2,1:T(8,128)(2,1)} reshape(bf16[8,4,2,192,1,128]{3,2,1,0,5,4:T(2,128)(2,1)} %copy.79) | data formatting | bytes 6291456 | tf_op jit(solution)/shard_map/reshape;reshape;reshape | solution.py:108
  187.9 3.9 %copy.81 = bf16[8,4,2,192,1,128]{5,3,2,1,0,4:T(8,128)(2,1)} copy(bf16[8,4,2,192,1,128]{5,3,1,0,2,4:T(8,128)(2,1)} %bitcast.125) | data formatting | bytes 6291456 | tf_op jit(solution)/shard_map/transpose | solution.py:26
  191.9 25.5 %while.17 = (s32[]{:T(128)}, f32[1,2,2,192]{3,1,2,0:T(2,128)S(1)}, f32[1,2,2,192]{3,1,2,0:T(2,128)S(1)}, f32[1,2,2,192,128]{4,3,2,1,0:T(8,128)S(1)}, s32[192]{0:...) while((s32[]{:T(128)}, f32[1,2,2,192]{3,1,2,0:T(2,128)S(1)}, ...), condition=%wide.region_5.6_spmd, body=%wide.region_0.5_spmd.sunk | while | flops 232147968 | bytes 8857645 | solution.py:128
  191.9 0.6 slice.57
  193.2 4.3 %conditional.2 = ((f32[1,2,2,192]{3,1,2,0:T(2,128)S(1)}, f32[1,2,2,192]{3,1,2,0:T(2,128)S(1)}, f32[1,2,2,192,128]{4,3,2,1,0:T(8,128)S(1)})) conditional(s32[]{:T(128)} %convert_element_type.91, (f32[1,2,2,192]{3,1,2,0:T(2,128)S(1)}, f32[1,2,2,192]{3,1,2,0:T(2,128)S(1)}, f32[1,2,2,192,128]{4,3,2,1,0:T(8,128)S(1)}) %tuple.61, (s32[]{:T(128)}, ...), branch_computations={%region_1.0_spmd, %region_2.4_spmd} | conditional | flops 232147968 | bytes 8857422 | solution.py:125
  193.2 0.1 broadcast_compare_fusion
  193.4 1.6 fusion
  195.0 0.9 fusion.4
  195.9 1.5 fusion.3
  197.5 0.6 slice.57
  198.8 0.6 slice.57
  200.1 0.6 slice.57
  201.5 0.6 slice.57
  202.8 0.6 slice.57
  204.1 0.6 slice.57
  205.4 0.6 slice.57
  206.8 0.6 slice.57
  208.1 0.6 slice.57
  209.4 0.6 slice.57
  210.7 0.6 slice.57
  212.1 0.6 slice.57
  213.4 0.6 slice.57
  214.7 0.6 slice.57
  216.0 0.6 slice.57
  217.4 0.3 multiply_reduce_fusion.1
  217.7 0.1 fusion.32
  217.9 1.3 convolution_convert_fusion.2
  219.3 4.0 %all-to-all-start = ((bf16[4,48,2048]{2,1,0:T(8,128)(2,1)}), bf16[4,48,2048]{2,1,0:T(8,128)(2,1)S(1)}, u32[]{:S(2)}, u32[]{:S(2)}) async-start(bf16[4,48,2048]{2,1,0:T(8,128)(2,1)} %bitcast.30), calls=%async_computation | async-start | bytes 1572864 | tf_op jit(solution)/shard_map/all_to_all | solution.py:40
  223.3 3.1 reduce_sum.78
  226.3 1.2 all_to_all.32
  227.6 5.9 %all-to-all-done = bf16[4,48,2048]{2,1,0:T(8,128)(2,1)S(1)} async-done(((bf16[4,48,2048]{2,1,0:T(8,128)(2,1)}), bf16[4,48,2048]{2,1,0:T(8,128)(2,1)S(1)}, u32[]{:S(2)}, u32[]{:S(2)}) %all-to-all-start) | async-done | bytes 786464 | tf_op jit(solution)/shard_map/all_to_all | solution.py:40
  233.4 0.9 copy-done.1
  234.3 72.2 %all-to-all-start.4 = ((bf16[64,4,2048]{2,1,0:T(4,128)(2,1)}), bf16[64,4,2048]{2,1,0:T(4,128)(2,1)S(1)}, u32[]{:S(2)}, u32[]{:S(2)}) async-start(bf16[64,4,2048]{2,1,0:T(4,128)(2,1)} %all_to_all.32), calls=%async_computation.4 | async-start | bytes 2097152 | tf_op jit(solution)/shard_map/all_to_all | solution.py:189
  306.7 0.1 reshape.226
  306.8 0.1 copy.90
  307.0 2.0 reduce_sum.74
  309.0 25.7 %all-to-all-done.4 = bf16[64,4,2048]{2,1,0:T(4,128)(2,1)S(1)} async-done(((bf16[64,4,2048]{2,1,0:T(4,128)(2,1)}), bf16[64,4,2048]{2,1,0:T(4,128)(2,1)S(1)}, u32[]{:S(2)}, u32[]{:S(2)}) %all-to-all-start.4) | async-done | bytes 1048608 | tf_op jit(solution)/shard_map/all_to_all | solution.py:189
  334.7 0.3 all_to_all.34
  335.0 1.1 gather_fusion
  336.1 0.5 reshape.225
  336.6 4.2 %multiply_reduce_fusion = bf16[96,2048]{1,0:T(8,128)(2,1)} fusion(bf16[96,2,2048]{2,1,0:T(2,128)(2,1)S(1)} %reshape.225, pred[96,2]{1,0:T(8,128)(4,1)S(1)} %copy.90, f32[96,2]{1,0:T(8,128)S(1)} %copy.85), kind=kLoop, calls=%fused_computation.33 | loop fusion | flops 1376256 | bytes 1180608 | tf_op jit(solution)/shard_map/reduce_sum | solution.py:191
  (68 shorter events, 1.3 us)
Async XLA Ops:
  7.2 210.8 %copy-start = (bf16[2,128,2048]{2,1,0:T(8,128)(2,1)S(1)}, bf16[2,128,2048]{2,1,0:T(8,128)(2,1)}, u32[]{:S(2)}) copy-start(bf16[2,128,2048]{2,1,0:T(8,128)(2,1)} %param.22) | copy-start | bytes 3145732
  7.2 77.8 %all-gather.7.cloned.1.call-start = ((), (), s32[]{:S(2)}) async-start(), calls=%async_computation.5 | async-start | bytes 1769472 | tf_op jit(solution)/shard_map/all_gather | solution.py:22
  19.9 88.8 %all-gather.11.cloned.1.call-start = ((), (), s32[]{:S(2)}) async-start(), calls=%async_computation.7 | async-start | bytes 1769472 | tf_op jit(solution)/shard_map/all_gather | solution.py:22
  30.1 136.7 %all-gather.9.cloned.1.call-start = ((), (), s32[]{:S(2)}) async-start(), calls=%async_computation.6 | async-start | bytes 4718592 | tf_op jit(solution)/shard_map/all_gather | solution.py:22
  87.5 53.1 %all-to-all-start.2 = ((bf16[4,256,2048]{2,1,0:T(8,128)(2,1)}), bf16[4,256,2048]{2,1,0:T(8,128)(2,1)}, u32[]{:S(2)}, u32[]{:S(2)}) async-start(bf16[4,256,2048]{2,1,0:T(8,128)(2,1)} %tile.10), calls=%async_computation.2 | async-start | bytes 8388608 | tf_op jit(solution)/shard_map/all_to_all | solution.py:171
  92.4 95.5 %all-gather.13.cloned.1.call-start = ((), (), s32[]{:S(2)}) async-start(), calls=%async_computation.8 | async-start | bytes 4718592 | tf_op jit(solution)/shard_map/all_gather | solution.py:22
  140.6 7.5 %copy-start.6 = (bf16[1,2048,896]{2,1,0:T(8,128)(2,1)S(1)}, bf16[1,2048,896]{2,1,0:T(8,128)(2,1)}, u32[]{:S(2)}) copy-start(bf16[1,2048,896]{2,1,0:T(8,128)(2,1)} %param.27) | copy-start | bytes 11010052
  148.1 7.4 %copy-start.7 = (bf16[1,896,2048]{2,1,0:T(8,128)(2,1)S(1)}, bf16[1,896,2048]{2,1,0:T(8,128)(2,1)}, u32[]{:S(2)}) copy-start(bf16[1,896,2048]{2,1,0:T(8,128)(2,1)} %param.29) | copy-start | bytes 11010052
  161.5 5.2 %copy-start.2 = (bf16[192,2,128]{2,1,0:T(2,128)(2,1)S(1)}, bf16[192,2,128]{2,1,0:T(2,128)(2,1)}, u32[]{:S(2)}) copy-start(bf16[192,2,128]{2,1,0:T(2,128)(2,1)} %param.17) | copy-start | bytes 294916
  161.5 57.7 %all-to-all-start.3 = ((bf16[4,256,2048]{2,1,0:T(8,128)(2,1)}), bf16[4,256,2048]{2,1,0:T(8,128)(2,1)}, u32[]{:S(2)}, u32[]{:S(2)}) async-start(bf16[4,256,2048]{2,1,0:T(8,128)(2,1)} %bitcast.122), calls=%async_computation.3 | async-start | bytes 8388608 | tf_op jit(solution)/shard_map/all_to_all | solution.py:40
  191.8 25.5 %copy-start.5 = (f32[2]{0:T(128)S(1)}, f32[2]{0:T(128)}, u32[]{:S(2)}) copy-start(f32[2]{0:T(128)} %param.20) | copy-start | bytes 28
  191.9 25.8 %copy-start.4 = (f32[128]{0:T(128)S(1)}, f32[128]{0:T(128)}, u32[]{:S(2)}) copy-start(f32[128]{0:T(128)} %param.21) | copy-start | bytes 1540
  219.3 14.2 %all-to-all-start = ((bf16[4,48,2048]{2,1,0:T(8,128)(2,1)}), bf16[4,48,2048]{2,1,0:T(8,128)(2,1)S(1)}, u32[]{:S(2)}, u32[]{:S(2)}) async-start(bf16[4,48,2048]{2,1,0:T(8,128)(2,1)} %bitcast.30), calls=%async_computation | async-start | bytes 1572864 | tf_op jit(solution)/shard_map/all_to_all | solution.py:40
  226.3 80.6 %copy-start.3 = (f32[96,2]{0,1:T(2,128)S(1)}, f32[96,2]{0,1:T(2,128)}, u32[]{:S(2)}) copy-start(f32[96,2]{0,1:T(2,128)} %param.26) | copy-start | bytes 2308
  233.4 0.9 copy-start.1
  234.3 100.4 %all-to-all-start.4 = ((bf16[64,4,2048]{2,1,0:T(4,128)(2,1)}), bf16[64,4,2048]{2,1,0:T(4,128)(2,1)S(1)}, u32[]{:S(2)}, u32[]{:S(2)}) async-start(bf16[64,4,2048]{2,1,0:T(4,128)(2,1)} %all_to_all.32), calls=%async_computation.4 | async-start | bytes 2097152 | tf_op jit(solution)/shard_map/all_to_all | solution.py:189
Sparse Core Ops, SparseCore 0:
  20.0 43.5 all-gather.6
  65.3 43.2 all-gather.10
  110.5 20.5 all-gather.8
  132.7 18.7 all-gather.12
